TPU v7x, 32 devices: a whole 2x2x4 slice. The times are simulated.
32 devices in a mesh: tp: 8 (over z, x), dp: 4 (over y, core).
Axes of the slice: x: 2, y: 2, z: 4, core: 2. Of those that a mesh axis runs over, the one named last changes fastest.
Arguments:
- tokens: bfloat16 [64, 4096], P(None, 'dp'), may hold values from -6 to 6
- recurrent_state: float32 [2, 64, 262144], P(None, 'dp', 'tp'), may hold values from -24 to 24
- pre_gain: float32 [2, 4096], P(None, 'dp'), may hold values from 0.1 to 1.9
- w_query: bfloat16 [2, 4096, 2048], P(None, 'dp', 'tp'), may hold values from -0.09375 to 0.09375
- w_key: bfloat16 [2, 4096, 2048], P(None, 'dp', 'tp'), may hold values from -0.09375 to 0.09375
- w_value: bfloat16 [2, 4096, 4096], P(None, 'dp', 'tp'), may hold values from -0.09375 to 0.09375
- w_gate: bfloat16 [2, 4096, 4096], P(None, 'dp', 'tp'), may hold values from -0.09375 to 0.09375
- w_decay: bfloat16 [2, 4096, 2048], P(None, 'dp', 'tp'), may hold values from -1 to 1
- decay_bias: float32 [2, 2048], P(None, 'tp'), may hold values from -5 to 3
- head_gain: float32 [2, 128], replicated, may hold values from 0.1 to 1.9
- w_out: bfloat16 [2, 4096, 4096], P(None, 'tp', 'dp'), may hold values from -0.09375 to 0.09375
- post_gain: float32 [2, 4096], P(None, 'dp'), may hold values from 0.1 to 1.9
Outputs:
- hidden_out: bfloat16 [64, 4096], P(None, 'dp')
- state_out: float32 [2, 64, 262144], P(None, 'dp', 'tp')
All inputs are finite; a program needn't handle non-finite values.
Results may differ from a plain program's by a relative error of at most 0.015.
Values may be sent and summed in bfloat16 or wider, within the bound.
A program may use at most 64 MiB of HBM per device.

v0:
```python
import jax
import jax.numpy as jnp
from jax import lax
from jax.sharding import PartitionSpec as P

D = 4096
KEY = 64
VAL = 128


epsilon = 1e-06


def local(
    tokens,
    recurrent_state,
    pre_gain,
    w_query,
    w_key,
    w_value,
    w_gate,
    w_decay,
    decay_bias,
    head_gain,
    w_out,
    post_gain,
):
    local_seqs = recurrent_state.shape[1]
    value_cols = recurrent_state.shape[2] // KEY
    heads_here = value_cols // VAL
    highest = lax.Precision.HIGHEST
    spread = (
        jnp.arange(value_cols, dtype=jnp.int32)[None, :] // VAL
        == jnp.arange(heads_here, dtype=jnp.int32)[:, None]
    ).astype(jnp.float32)

    def spread_heads(vectors):
        shaped = vectors.astype(jnp.float32).reshape(local_seqs, heads_here, KEY)
        return jnp.einsum("bhk,hc->bck", shaped, spread, precision=highest)

    residual = tokens
    new_states = []
    for section_index in range(2):
        wide_float = residual.astype(jnp.float32)
        squares_part = jnp.sum(wide_float * wide_float, axis=1)
        normed = (wide_float * pre_gain[section_index]).astype(jnp.bfloat16)
        partials = tuple(
            (
                jnp.dot(normed, weights[section_index], preferred_element_type=jnp.float32)
                for weights in (w_query, w_key, w_value, w_gate, w_decay)
            )
        )
        summed = lax.psum_scatter(partials + (squares_part,), "dp", scatter_dimension=0, tiled=True)
        projected = summed[:5]
        own_squares = summed[5]
        row_scale = lax.rsqrt(own_squares / D + epsilon)[:, None]
        query_part = (projected[0] * row_scale).astype(jnp.bfloat16)
        key_part = (projected[1] * row_scale).astype(jnp.bfloat16)
        values_own = projected[2] * row_scale
        gate_pre = projected[3] * row_scale
        log_decay = jax.nn.log_sigmoid(projected[4] * row_scale + decay_bias[section_index]) / 16.0
        query_cols = spread_heads(query_part)
        key_cols = spread_heads(key_part)
        decay_cols = jnp.exp(spread_heads(log_decay))
        old_state = recurrent_state[section_index].reshape(local_seqs, value_cols, KEY)
        new_state = decay_cols * old_state + key_cols * values_own[:, :, None]
        readout = jnp.sum(query_cols * new_state, axis=2) * KEY ** (-0.5)
        head_mean = jnp.mean(
            (readout * readout).reshape(local_seqs, heads_here, VAL), axis=2, keepdims=True
        )
        scaled = (
            readout.reshape(local_seqs, heads_here, VAL)
            * lax.rsqrt(head_mean + epsilon)
            * head_gain[section_index]
        )
        mixed = (scaled.reshape(local_seqs, value_cols) * jax.nn.silu(gate_pre)).astype(
            jnp.bfloat16
        )
        out_weight = w_out[section_index]
        partial_out = jnp.dot(
            lax.all_gather(mixed, "dp", axis=0, tiled=True),
            out_weight,
            preferred_element_type=jnp.float32,
        )
        out_rows = lax.psum(partial_out, "tp")
        out_squares = lax.psum(jnp.sum(out_rows * out_rows, axis=1), "dp")
        residual = (
            wide_float
            + out_rows * lax.rsqrt(out_squares / D + epsilon)[:, None] * post_gain[section_index]
        ).astype(jnp.bfloat16)
        new_states.append(new_state.reshape(local_seqs, value_cols * KEY))
    return (residual, jnp.stack(new_states))


def solution(mesh):
    in_specs = (
        P(None, "dp"),
        P(None, "dp", "tp"),
        P(None, "dp"),
        P(None, "dp", "tp"),
        P(None, "dp", "tp"),
        P(None, "dp", "tp"),
        P(None, "dp", "tp"),
        P(None, "dp", "tp"),
        P(None, "tp"),
        P(),
        P(None, "tp", "dp"),
        P(None, "dp"),
    )
    out_specs = (P(None, "dp"), P(None, "dp", "tp"))
    return jax.shard_map(local, mesh=mesh, in_specs=in_specs, out_specs=out_specs, check_vma=False)
```

profile of v0, /device:TPU:0, one launch (start us, length us, event | category | flops | bytes accessed | tf_op | source)
XLA Modules:
  0.0 412.4 jit_solution(11796743993679151280)
XLA Ops:
  7.2 0.9 fusion.85
  8.1 2.0 fusion.32
  10.1 1.9 fusion.30
  12.2 1.9 fusion.28
  14.2 0.9 fusion.14
  15.2 2.2 fusion.12
  17.5 0.1 fusion.41
  17.6 3.9 fusion.83
  21.5 3.0 reshape_squeeze.6
  24.5 3.8 copy.18
  28.3 8.4 %all-reduce = f32[64]{0:T(128)S(1)} all-reduce(f32[64]{0:T(128)S(1)} %fusion.41), channel_id=3, replica_groups=mesh['tp'=8,'dp'=4] {'dp'}, use_global_device_ids=true, to_apply=%region_2.3.clone | all-reduce | flops 64 | bytes 512
  36.7 0.6 dynamic-slice
  38.1 16.7 %reduce-scatter.13.cloned.1.call-done = f32[16,256]{1,0:T(8,128)} async-done(((f32[64,256]{1,0:T(8,128)}), f32[16,256]{1,0:T(8,128)}) %reduce-scatter.13.cloned.1.call-update) | async-done | bytes 16400 | tf_op jit(solution)/shard_map/reduce_scatter | solution.py:53
  54.7 22.0 %reduce-scatter.15.cloned.1.call-done = f32[16,256]{1,0:T(8,128)} async-done(((f32[64,256]{1,0:T(8,128)}), f32[16,256]{1,0:T(8,128)}) %reduce-scatter.15.cloned.1.call-update) | async-done | bytes 16400 | tf_op jit(solution)/shard_map/reduce_scatter | solution.py:53
  76.7 0.8 multiply_convert_fusion.3
  77.7 0.1 reshape.105
  77.8 0.1 reshape.103
  77.8 2.4 fusion.79
  80.2 19.1 %reduce-scatter.17.cloned.1.call-done = f32[16,512]{1,0:T(8,128)} async-done(((f32[64,512]{1,0:T(8,128)}), f32[16,512]{1,0:T(8,128)}) %reduce-scatter.17.cloned.1.call-update) | async-done | bytes 32784 | tf_op jit(solution)/shard_map/reduce_scatter | solution.py:53
  99.3 0.8 broadcast_multiply_fusion.1
  100.1 2.7 fusion.2
  102.9 0.5 fusion.3
  103.4 0.1 reduce_sum.74
  103.5 17.7 %reduce-scatter.19.cloned.1.call-done = f32[16,512]{1,0:T(8,128)} async-done(((f32[64,512]{1,0:T(8,128)}), f32[16,512]{1,0:T(8,128)}) %reduce-scatter.19.cloned.1.call-update) | async-done | bytes 32784 | tf_op jit(solution)/shard_map/reduce_scatter | solution.py:53
  121.3 0.9 fusion.61
  122.2 5.2 %all_gather.6 = bf16[64,512]{1,0:T(8,128)(2,1)S(1)} all-gather(bf16[16,512]{1,0:T(8,128)(2,1)S(1)} %fusion.61), channel_id=1, replica_groups=mesh['tp'=8,'dp'=4] {'dp'}, dimensions={0}, use_global_device_ids=true | all-gather | bytes 81920 | tf_op jit(solution)/shard_map/all_gather | solution.py:81
  127.4 2.2 fusion.10
  129.7 4.2 %reshape_squeeze.7 = f32[16,512,64]{2,1,0:T(8,128)} reshape(f32[1,16,32768]{2,1,0:T(8,128)} %get-tuple-element.4) | data formatting | bytes 4194304 | tf_op jit(solution)/shard_map/reshape;squeeze | solution.py:65
  133.9 3.9 copy.19
  137.8 2.8 copy.20
  140.6 4.1 stack_reshape.6
  144.7 56.1 %all-reduce.5.cloned.1.call-done = f32[64,1024]{1,0:T(8,128)} async-done(((f32[64,1024]{1,0:T(8,128)}), f32[64,1024]{1,0:T(8,128)}) %all-reduce.5.cloned.1.call-update) | async-done | bytes 262160 | tf_op jit(solution)/shard_map/psum | solution.py:85
  200.8 1.1 multiply_reduce_fusion.1
  201.9 5.7 %psum.29 = f32[64]{0:T(128)S(1)} all-reduce(f32[64]{0:T(128)S(1)} %multiply_reduce_fusion.1), channel_id=1, replica_groups=mesh['tp'=8,'dp'=4] {'dp'}, use_global_device_ids=true, to_apply=%region_11.12 | all-reduce | flops 64 | bytes 512 | tf_op jit(solution)/shard_map/psum | solution.py:86
  207.5 1.2 fusion.44
  208.7 0.9 fusion.26
  209.7 6.6 %all-reduce.1 = f32[64]{0:T(128)S(1)} all-reduce(f32[64]{0:T(128)S(1)} %get-tuple-element.2), channel_id=9, replica_groups=mesh['tp'=8,'dp'=4] {'dp'}, use_global_device_ids=true, to_apply=%region_14.15.clone | all-reduce | flops 64 | bytes 512
  216.3 0.8 fusion.24
  217.2 1.9 fusion.22
  219.1 2.2 fusion.8
  221.5 2.2 fusion.6
  223.7 5.1 %reduce-scatter.21.cloned.1.call-done = f32[16,256]{1,0:T(8,128)} async-done(((f32[64,256]{1,0:T(8,128)}), f32[16,256]{1,0:T(8,128)}) %reduce-scatter.21.cloned.1.call-update) | async-done | bytes 16400 | tf_op jit(solution)/shard_map/reduce_scatter | solution.py:53
  228.8 22.0 %reduce-scatter.23.cloned.1.call-done = f32[16,256]{1,0:T(8,128)} async-done(((f32[64,256]{1,0:T(8,128)}), f32[16,256]{1,0:T(8,128)}) %reduce-scatter.23.cloned.1.call-update) | async-done | bytes 16400 | tf_op jit(solution)/shard_map/reduce_scatter | solution.py:53
  250.8 22.0 %reduce-scatter.25.cloned.1.call-done = f32[16,256]{1,0:T(8,128)} async-done(((f32[64,256]{1,0:T(8,128)}), f32[16,256]{1,0:T(8,128)}) %reduce-scatter.25.cloned.1.call-update) | async-done | bytes 16400 | tf_op jit(solution)/shard_map/reduce_scatter | solution.py:53
  272.8 0.8 multiply_convert_fusion.1
  273.7 2.4 fusion.75
  276.1 0.1 reshape.108
  276.2 0.1 reshape.106
  276.3 19.1 %reduce-scatter.27.cloned.1.call-done = f32[16,512]{1,0:T(8,128)} async-done(((f32[64,512]{1,0:T(8,128)}), f32[16,512]{1,0:T(8,128)}) %reduce-scatter.27.cloned.1.call-update) | async-done | bytes 32784 | tf_op jit(solution)/shard_map/reduce_scatter | solution.py:53
  295.3 0.8 broadcast_multiply_fusion
  296.2 2.8 fusion
  298.9 0.5 fusion.1
  299.4 2.8 copy.21
  302.2 0.1 reduce_sum.78
  302.3 15.1 %reduce-scatter.29.cloned.1.call-done = f32[16,512]{1,0:T(8,128)} async-done(((f32[64,512]{1,0:T(8,128)}), f32[16,512]{1,0:T(8,128)}) %reduce-scatter.29.cloned.1.call-update) | async-done | bytes 32784 | tf_op jit(solution)/shard_map/reduce_scatter | solution.py:53
  317.5 0.9 fusion.58
  318.3 5.2 %all_gather.7 = bf16[64,512]{1,0:T(8,128)(2,1)S(1)} all-gather(bf16[16,512]{1,0:T(8,128)(2,1)S(1)} %fusion.58), channel_id=1, replica_groups=mesh['tp'=8,'dp'=4] {'dp'}, dimensions={0}, use_global_device_ids=true | all-gather | bytes 81920 | tf_op jit(solution)/shard_map/all_gather | solution.py:81
  323.6 2.2 fusion.4
  325.8 4.0 stack_reshape.7
  329.9 3.9 pad_maximum_fusion
  333.7 63.3 %all-reduce.7.cloned.1.call-done = f32[64,1024]{1,0:T(8,128)} async-done(((f32[64,1024]{1,0:T(8,128)}), f32[64,1024]{1,0:T(8,128)}) %all-reduce.7.cloned.1.call-update) | async-done | bytes 262160 | tf_op jit(solution)/shard_map/psum | solution.py:85
  397.1 1.1 multiply_reduce_fusion
  398.1 5.7 %psum.31 = f32[64]{0:T(128)S(1)} all-reduce(f32[64]{0:T(128)S(1)} %multiply_reduce_fusion), channel_id=1, replica_groups=mesh['tp'=8,'dp'=4] {'dp'}, use_global_device_ids=true, to_apply=%region_23.24 | all-reduce | flops 64 | bytes 512 | tf_op jit(solution)/shard_map/psum | solution.py:86
  403.8 1.7 fusion.45
  (63 shorter events, 1.3 us)
Async XLA Ops:
  7.2 7.0 %copy-start.1 = (bf16[64,1024]{1,0:T(8,128)(2,1)S(1)}, bf16[64,1024]{1,0:T(8,128)(2,1)}, u32[]{:S(2)}) copy-start(bf16[64,1024]{1,0:T(8,128)(2,1)} %param.12) | copy-start | bytes 393220
  7.2 7.0 %copy-start.5 = (bf16[2,1024,512]{2,1,0:T(8,128)(2,1)S(1)}, bf16[2,1024,512]{2,1,0:T(8,128)(2,1)}, u32[]{:S(2)}) copy-start(bf16[2,1024,512]{2,1,0:T(8,128)(2,1)} %param.17) | copy-start | bytes 6291460
  7.2 30.9 %reduce-scatter.11.cloned.1.call-start = ((), (), s32[]{:S(2)}) async-start(), calls=%async_computation.10 | async-start | bytes 81920 | tf_op jit(solution)/shard_map/reduce_scatter | solution.py:53
  10.1 44.6 %reduce-scatter.13.cloned.1.call-start = ((), (), s32[]{:S(2)}) async-start(), calls=%async_computation.11 | async-start | bytes 81920 | tf_op jit(solution)/shard_map/reduce_scatter | solution.py:53
  12.1 64.6 %reduce-scatter.15.cloned.1.call-start = ((), (), s32[]{:S(2)}) async-start(), calls=%async_computation.12 | async-start | bytes 81920 | tf_op jit(solution)/shard_map/reduce_scatter | solution.py:53
  14.1 85.1 %reduce-scatter.17.cloned.1.call-start = ((), (), s32[]{:S(2)}) async-start(), calls=%async_computation.13 | async-start | bytes 163840 | tf_op jit(solution)/shard_map/reduce_scatter | solution.py:53
  15.2 106.0 %reduce-scatter.19.cloned.1.call-start = ((), (), s32[]{:S(2)}) async-start(), calls=%async_computation.14 | async-start | bytes 163840 | tf_op jit(solution)/shard_map/reduce_scatter | solution.py:53
  17.4 183.4 %all-reduce.5.cloned.1.call-start = ((), (), s32[]{:S(2)}) async-start(), calls=%async_computation.15 | async-start | bytes 524288 | tf_op jit(solution)/shard_map/psum | solution.py:85
  24.5 12.2 %copy-start.3 = (f32[2,256]{1,0:T(2,128)S(1)}, f32[2,256]{1,0:T(2,128)}, u32[]{:S(2)}) copy-start(f32[2,256]{1,0:T(2,128)} %param.20) | copy-start | bytes 6148
  24.5 12.2 %copy-start.4 = (f32[2,128]{1,0:T(2,128)S(1)}, f32[2,128]{1,0:T(2,128)}, u32[]{:S(2)}) copy-start(f32[2,128]{1,0:T(2,128)} %param.21) | copy-start | bytes 3076
  24.5 12.3 %copy-start.8 = (u32[32]{0:T(128)S(1)}, u32[32]{0:T(128)}, u32[]{:S(2)}) copy-start(u32[32]{0:T(128)} %constant.51) | copy-start | bytes 388
  129.6 99.2 %reduce-scatter.21.cloned.1.call-start = ((), (), s32[]{:S(2)}) async-start(), calls=%async_computation.16 | async-start | bytes 81920 | tf_op jit(solution)/shard_map/reduce_scatter | solution.py:53
  133.9 3.9 copy-start.2
  140.6 68.1 %copy-start.6 = (bf16[2,1024,256]{2,1,0:T(8,128)(2,1)S(1)}, bf16[2,1024,256]{2,1,0:T(8,128)(2,1)}, u32[]{:S(2)}) copy-start(bf16[2,1024,256]{2,1,0:T(8,128)(2,1)} %param.15) | copy-start | bytes 3145732
  140.6 75.7 %copy-start.7 = (bf16[2,1024,256]{2,1,0:T(8,128)(2,1)S(1)}, bf16[2,1024,256]{2,1,0:T(8,128)(2,1)}, u32[]{:S(2)}) copy-start(bf16[2,1024,256]{2,1,0:T(8,128)(2,1)} %param.19) | copy-start | bytes 3145732
  209.6 41.2 %reduce-scatter.23.cloned.1.call-start = ((), (), s32[]{:S(2)}) async-start(), calls=%async_computation.17 | async-start | bytes 81920 | tf_op jit(solution)/shard_map/reduce_scatter | solution.py:53
  217.1 55.7 %reduce-scatter.25.cloned.1.call-start = ((), (), s32[]{:S(2)}) async-start(), calls=%async_computation.18 | async-start | bytes 81920 | tf_op jit(solution)/shard_map/reduce_scatter | solution.py:53
  219.1 76.2 %reduce-scatter.27.cloned.1.call-start = ((), (), s32[]{:S(2)}) async-start(), calls=%async_computation.19 | async-start | bytes 163840 | tf_op jit(solution)/shard_map/reduce_scatter | solution.py:53
  221.3 96.1 %reduce-scatter.29.cloned.1.call-start = ((), (), s32[]{:S(2)}) async-start(), calls=%async_computation.20 | async-start | bytes 163840 | tf_op jit(solution)/shard_map/reduce_scatter | solution.py:53
  223.6 173.4 %all-reduce.7.cloned.1.call-start = ((), (), s32[]{:S(2)}) async-start(), calls=%async_computation.21 | async-start | bytes 524288 | tf_op jit(solution)/shard_map/psum | solution.py:85
  325.8 4.0 copy-start
Sparse Core Ops, SparseCore 0:
  10.4 22.2 reduce-scatter.10
  35.1 19.5 reduce-scatter.12
  57.1 19.5 reduce-scatter.14
  79.6 19.6 reduce-scatter.16
  101.5 19.6 reduce-scatter.18
  129.8 70.9 all-reduce.4
  209.7 19.0 reduce-scatter.20
  231.2 19.5 reduce-scatter.22
  253.2 19.5 reduce-scatter.24
  275.6 19.6 reduce-scatter.26
  297.8 19.6 reduce-scatter.28
  326.0 71.0 all-reduce.6
where the time goes:
time: 414 us; the launch traced here: 412 us
  waiting for transfers between devices  278 us (67%)
  blocking collectives  36.8 us (9%)
  local copies, waits for them, and re-layouts  34.7 us (8%)
  matrix products  32.5 us (8%)
  between operations  15.1 us (4%)
  other arithmetic  14.5 us (4%)
    reduce_scatter x10, waiting for transfers between devices, local(): lax.psum_scatter(partials + (squares_part,), 'dp', scatter_dimension=0, t...  159 us
    psum x2, waiting for transfers between devices, local(): out_rows = lax.psum(partial_out, 'tp')  119 us
    dot_general x10, matrix products, local(): jnp.dot(normed, weights[section_index], preferred_element_type=jnp.float32)  16.9 us
    unnamed x2, blocking collectives  15 us
    another operation x4, local copies, waits for them, and re-layouts, local(): recurrent_state[section_index].reshape(local_seqs, value_cols, KEY)  14.9 us
    psum x2, blocking collectives, local(): out_squares = lax.psum(jnp.sum(out_rows * out_rows, axis=1), 'dp')  11.3 us
    dot_general x6, matrix products, spread_heads(): return jnp.einsum('bhk,hc->bck', shaped, spread, precision=highest)  11.2 us
    all_gather x2, blocking collectives, local(): lax.all_gather(mixed, 'dp', axis=0, tiled=True)  10.5 us
  transfers between devices with their start and end apart: 12, of which 11 were waited for; matrix products, arithmetic and copies ran while one was open for 16% of the time, Pallas kernels for 0%

commit v1 on v0

v1 whole, which is shorter than its diff:
```python
import functools

import jax
import jax.numpy as jnp
from jax import lax
from jax.experimental import pallas as pl
from jax.experimental.pallas import tpu as pltpu
from jax.sharding import PartitionSpec as P

KEY = 64
VAL = 128
LANES = 128
epsilon = 1e-06
MESH = pl.DeviceIdType.MESH
F32 = jnp.float32
BF16 = jnp.bfloat16


def pad(width):
    return -(-width // LANES) * LANES


def kernel(
    dp, tp, qk, vw, tile,
    tok, st, pre, wq, wk, wv, wg, wd, bias, hgain, wo, post,
    hid, sto,
    W, WO, S, xf, nrm, part, rbuf, sqa, sqb, psum,
    qd2, dec2, k2, vv, base, sg, mg, obuf, rb, sqo, sqr, xg,
    wsem, wosem, ssem, osem, sA, rA, sQ, rQ, sB, rB, sC, rC, sR, rR, sG, rG,
):
    me_dp = lax.axis_index("dp")
    me_tp = lax.axis_index("tp")
    seqs = tok.shape[0]
    rows = seqs // dp
    orows = seqs // tp
    feats = tok.shape[1] * dp
    heads = vw // VAL
    tiles = W.shape[2] // tile
    q_at, k_at, d_at = 0, pad(qk), 2 * pad(qk)
    v_at = 3 * pad(qk)
    g_at = v_at + vw
    sections = ((wq, q_at, pad(qk)), (wk, k_at, pad(qk)), (wd, d_at, pad(qk)), (wv, v_at, vw), (wg, g_at, vw))

    def dp_peer(k):
        return lax.rem(me_dp + k, dp)

    def tp_peer(k):
        return lax.rem(me_tp + k, tp)

    for k in range(1, dp):
        pl.semaphore_signal(pltpu.get_barrier_semaphore(), inc=1, device_id={"dp": dp_peer(k)}, device_id_type=MESH)
    for k in range(1, tp):
        pl.semaphore_signal(pltpu.get_barrier_semaphore(), inc=1, device_id={"tp": tp_peer(k)}, device_id_type=MESH)

    def weight_copy(b, n):
        ref, at, width = sections[n]
        return pltpu.make_async_copy(ref.at[b], W.at[b, :, pl.ds(at, width)], wsem.at[b, n])

    def state_in(b):
        return pltpu.make_async_copy(st.at[b], S.at[b], ssem.at[b])

    def state_out(b):
        return pltpu.make_async_copy(S.at[b], sto.at[b], osem.at[b])

    def wo_copy(b):
        return pltpu.make_async_copy(wo.at[b], WO.at[b], wosem.at[b])

    for b in range(2):
        for n in range(5):
            weight_copy(b, n).start()
        state_in(b).start()
        wo_copy(b).start()

    xf[...] = tok[...].astype(F32)
    lane = lax.broadcasted_iota(jnp.int32, (LANES, LANES), 1)
    depth = lax.broadcasted_iota(jnp.int32, (LANES, LANES), 0)
    reducer = (depth // KEY == lane % 2).astype(F32).astype(BF16)
    lane_row = lax.broadcasted_iota(jnp.int32, (rows, LANES), 1)
    pair_of = lane_row // 2
    low_half = lane_row < KEY
    pairs = VAL // 2

    pl.semaphore_wait(pltpu.get_barrier_semaphore(), dp - 1 + tp - 1)

    def remote(src, dst, send, recv, axis, peer):
        return pltpu.make_async_remote_copy(
            src_ref=src, dst_ref=dst, send_sem=send, recv_sem=recv,
            device_id={axis: peer}, device_id_type=MESH,
        )

    def copy_A(b, t, k):
        return remote(part.at[b, t, dp_peer(k)], rbuf.at[b, t, k], sA.at[b, t, k], rA.at[b, t, k], "dp", dp_peer(k))

    def copy_Q(b, k):
        return remote(sqa.at[b, dp_peer(k)], sqb.at[b, k], sQ.at[b, k], rQ.at[b, k], "dp", dp_peer(k))

    def copy_B(b, k):
        return remote(mg.at[b, me_dp], mg.at[b, me_dp], sB.at[b, k], rB.at[b, k], "dp", dp_peer(k))

    def wait_B(b, k):
        src = lax.rem(me_dp + dp - k, dp)
        remote(mg.at[b, src], mg.at[b, src], sB.at[b, k], rB.at[b, k], "dp", dp_peer(k)).wait_recv()

    def copy_C(b, k):
        return remote(obuf.at[b, tp_peer(k)], rb.at[b, k], sC.at[b, k], rC.at[b, k], "tp", tp_peer(k))

    def copy_R(b, k):
        return remote(sqo.at[b], sqr.at[b, k], sR.at[b, k], rR.at[b, k], "dp", dp_peer(k))

    def copy_G(b, k):
        return remote(xg.at[b, me_tp], xg.at[b, me_tp], sG.at[b, k], rG.at[b, k], "tp", tp_peer(k))

    def wait_G(b, k):
        src = lax.rem(me_tp + tp - k, tp)
        remote(xg.at[b, src], xg.at[b, src], sG.at[b, k], rG.at[b, k], "tp", tp_peer(k)).wait_recv()

    def block(b, carry):
        x = xf[...]
        squares = jnp.sum(x * x, axis=1, keepdims=True)
        sqa[b] = jnp.broadcast_to(squares, (seqs, LANES)).reshape(dp, rows, LANES)
        nrm[...] = (x * pre[pl.ds(b, 1), :]).astype(BF16)
        for k in range(1, dp):
            copy_Q(b, k).start()
        for n in range(5):
            weight_copy(b, n).wait()

        def project(t, c):
            cols = pl.ds(pl.multiple_of(t * tile, tile), tile)
            y = jnp.dot(nrm[...], W[b, :, cols], preferred_element_type=F32)
            part[b, t] = y.reshape(dp, rows, tile).astype(BF16)
            for k in range(1, dp):
                copy_A(b, t, k).start()
            return c

        lax.fori_loop(0, tiles, project, 0)

        total_sq = sqa[b, me_dp]
        for k in range(1, dp):
            copy_Q(b, k).wait_recv()
            total_sq = total_sq + sqb[b, k]
        row_scale = lax.rsqrt(total_sq[:, :1] / feats + epsilon)

        def collect(t, c):
            total = part[b, t, me_dp].astype(F32)
            for k in range(1, dp):
                copy_A(b, t, k).wait_recv()
                total = total + rbuf[b, t, k].astype(F32)
            psum[t] = total * row_scale
            return c

        lax.fori_loop(0, tiles, collect, 0)

        def piece(at, width):
            return psum[at // tile, :, pl.ds(at % tile, width)]

        bias_row = bias[pl.ds(b, 1), :]
        for h in range(heads):
            query = piece(q_at + h * KEY, KEY).astype(BF16).astype(F32)
            key_vec = piece(k_at + h * KEY, KEY).astype(BF16).astype(F32)
            z = piece(d_at + h * KEY, KEY) + bias_row[:, h * KEY : (h + 1) * KEY]
            log_sig = jnp.minimum(z, 0.0) - jnp.log(1.0 + jnp.exp(-jnp.abs(z)))
            decay = jnp.exp(log_sig / 16.0)
            value = piece(v_at + h * VAL, VAL)
            gate = piece(g_at + h * VAL, VAL)
            qd = query * decay
            qd2[h] = jnp.concatenate([qd, qd], axis=1)
            dec2[h] = jnp.concatenate([decay, decay], axis=1)
            k2[h] = jnp.concatenate([key_vec, key_vec], axis=1)
            vv[h] = value
            base[h] = jnp.sum(query * key_vec, axis=1, keepdims=True) * value
            sg[h] = gate / (1.0 + jnp.exp(-gate))

        state_in(b).wait()

        def readout(h, c):
            at = pl.multiple_of(h * VAL * KEY, LANES)
            qd = qd2[h]
            prods = jnp.concatenate(
                [S[b, :, pl.ds(at + j * LANES, LANES)] * qd for j in range(pairs)], axis=0
            ).astype(BF16)
            sums = jnp.dot(prods, reducer, preferred_element_type=F32)
            acc = base[h]
            for j in range(pairs):
                acc = acc + jnp.where(pair_of == j, sums[j * rows : (j + 1) * rows], 0.0)
            read = acc * KEY ** (-0.5)
            mean = jnp.mean(read * read, axis=1, keepdims=True)
            mixed = read * lax.rsqrt(mean + epsilon) * hgain[pl.ds(b, 1), :] * sg[h]
            mg[b, me_dp, :, pl.ds(pl.multiple_of(h * VAL, VAL), VAL)] = mixed.astype(BF16)
            return c

        lax.fori_loop(0, heads, readout, 0)
        for k in range(1, dp):
            copy_B(b, k).start()
        wo_copy(b).wait()
        for k in range(1, dp):
            wait_B(b, k)
        out = jnp.dot(mg[b].reshape(seqs, vw), WO[b], preferred_element_type=F32)
        obuf[b] = out.reshape(tp, orows, out.shape[1]).astype(BF16)
        for k in range(1, tp):
            copy_C(b, k).start()

        def update(h, c):
            at = pl.multiple_of(h * VAL * KEY, LANES)
            decay, key_vec, value = dec2[h], k2[h], vv[h]
            for j in range(pairs):
                here = pl.ds(at + j * LANES, LANES)
                spread = jnp.where(low_half, value[:, 2 * j : 2 * j + 1], value[:, 2 * j + 1 : 2 * j + 2])
                S[b, :, here] = decay * S[b, :, here] + key_vec * spread
            return c

        lax.fori_loop(0, heads, update, 0)
        state_out(b).start()

        total = obuf[b, me_tp].astype(F32)
        for k in range(1, tp):
            copy_C(b, k).wait_recv()
            total = total + rb[b, k].astype(F32)
        own_sq = jnp.broadcast_to(jnp.sum(total * total, axis=1, keepdims=True), (orows, LANES))
        sqo[b] = own_sq
        for k in range(1, dp):
            copy_R(b, k).start()
        mine = xf[pl.ds(pl.multiple_of(me_tp * orows, orows), orows), :]
        gained = total * post[pl.ds(b, 1), :]
        for k in range(1, dp):
            copy_R(b, k).wait_recv()
            own_sq = own_sq + sqr[b, k]
        out_scale = lax.rsqrt(own_sq[:, :1] / feats + epsilon)
        xg[b, me_tp] = (mine + gained * out_scale).astype(BF16)
        for k in range(1, tp):
            copy_G(b, k).start()
        for k in range(1, tp):
            wait_G(b, k)
        xf[...] = xg[b].astype(F32).reshape(seqs, xf.shape[1])

        for k in range(1, dp):
            copy_Q(b, k).wait_send()
            copy_B(b, k).wait_send()
            copy_R(b, k).wait_send()

        def drain(t, c):
            for k in range(1, dp):
                copy_A(b, t, k).wait_send()
            return c

        lax.fori_loop(0, tiles, drain, 0)
        for k in range(1, tp):
            copy_C(b, k).wait_send()
            copy_G(b, k).wait_send()
        return carry

    lax.fori_loop(0, 2, block, 0)
    hid[...] = xf[...].astype(BF16)
    for b in range(2):
        state_out(b).wait()


def solution(mesh):
    dp, tp = mesh.shape["dp"], mesh.shape["tp"]

    def local(tok, st, pre, wq, wk, wv, wg, wd, bias, hgain, wo, post):
        seqs, width = tok.shape
        rows, orows = seqs // dp, seqs // tp
        qk, vw = wq.shape[2], wv.shape[2]
        if pad(qk) != qk:
            fill = ((0, 0), (0, 0), (0, pad(qk) - qk))
            wq, wk, wd = (jnp.pad(w, fill) for w in (wq, wk, wd))
        heads = vw // VAL
        total = 3 * pad(qk) + 2 * vw
        tile = 2 * LANES if total % (2 * LANES) == 0 and pad(qk) % (2 * LANES) == 0 else LANES
        tiles = total // tile
        vmem = pl.BlockSpec(memory_space=pltpu.VMEM)
        hbm = pl.BlockSpec(memory_space=pl.ANY)
        dma = pltpu.SemaphoreType.DMA
        per_head = pltpu.VMEM((heads, rows, LANES), F32)
        return pl.pallas_call(
            functools.partial(kernel, dp, tp, qk, vw, tile),
            out_shape=(
                jax.ShapeDtypeStruct(tok.shape, BF16),
                jax.ShapeDtypeStruct(st.shape, F32),
            ),
            in_specs=[vmem, hbm, vmem, hbm, hbm, hbm, hbm, hbm, vmem, vmem, hbm, vmem],
            out_specs=(vmem, hbm),
            scratch_shapes=[
                pltpu.VMEM((2, width, total), BF16),
                pltpu.VMEM((2,) + wo.shape[1:], BF16),
                pltpu.VMEM(st.shape, F32),
                pltpu.VMEM((seqs, width), F32),
                pltpu.VMEM((seqs, width), BF16),
                pltpu.VMEM((2, tiles, dp, rows, tile), BF16),
                pltpu.VMEM((2, tiles, dp, rows, tile), BF16),
                pltpu.VMEM((2, dp, rows, LANES), F32),
                pltpu.VMEM((2, dp, rows, LANES), F32),
                pltpu.VMEM((tiles, rows, tile), F32),
                per_head, per_head, per_head, per_head, per_head, per_head,
                pltpu.VMEM((2, dp, rows, vw), BF16),
                pltpu.VMEM((2, tp, orows, width), BF16),
                pltpu.VMEM((2, tp, orows, width), BF16),
                pltpu.VMEM((2, orows, LANES), F32),
                pltpu.VMEM((2, dp, orows, LANES), F32),
                pltpu.VMEM((2, tp, orows, width), BF16),
                dma((2, 5)), dma((2,)), dma((2,)), dma((2,)),
                dma((2, tiles, dp)), dma((2, tiles, dp)),
                dma((2, dp)), dma((2, dp)),
                dma((2, dp)), dma((2, dp)),
                dma((2, tp)), dma((2, tp)),
                dma((2, dp)), dma((2, dp)),
                dma((2, tp)), dma((2, tp)),
            ],
            compiler_params=pltpu.CompilerParams(
                collective_id=0, has_side_effects=True, vmem_limit_bytes=60 * 2**20
            ),
        )(tok, st, pre, wq, wk, wv, wg, wd, bias, hgain, wo, post)

    in_specs = (
        P(None, "dp"),
        P(None, "dp", "tp"),
        P(None, "dp"),
        P(None, "dp", "tp"),
        P(None, "dp", "tp"),
        P(None, "dp", "tp"),
        P(None, "dp", "tp"),
        P(None, "dp", "tp"),
        P(None, "tp"),
        P(),
        P(None, "tp", "dp"),
        P(None, "dp"),
    )
    out_specs = (P(None, "dp"), P(None, "dp", "tp"))
    return jax.shard_map(local, mesh=mesh, in_specs=in_specs, out_specs=out_specs, check_vma=False)
```

time: 414 us -> 60.5 us (0.15)
  waiting for transfers between devices: 278 us -> 0 us
  Pallas kernels: 0 us -> 53.6 us
  blocking collectives: 36.8 us -> 0 us
  matrix products: 32.5 us -> 0 us
  local copies, waits for them, and re-layouts: 34.7 us -> 6.04 us
  other arithmetic: 14.5 us -> 0 us
  between operations: 15.1 us -> 0.64 us
    reduce_scatter x10 -> x0, waiting for transfers between devices: 159 us -> none  [local(): lax.psum_scatter(partials + (squares_part,), 'dp', scatter_dimension=0, t...]
    psum x2 -> x0, waiting for transfers between devices: 119 us -> none  [local(): out_rows = lax.psum(partial_out, 'tp')]
    pallas_call x0 -> x1, Pallas kernels: none -> 53.6 us  [local(): pl.pallas_call(functools.partial(kernel, dp, tp, qk, vw, tile), out_shape...]
    dot_general x18 -> x0, matrix products: 32.5 us -> none  [the longest x10 16.9 us: local(): jnp.dot(normed, weights[section_index], preferred_element_type=jnp.float32)]
    another operation x6 -> x0, local copies, waits for them, and re-layouts: 23 us -> none  [the longest x4 14.9 us: local(): recurrent_state[section_index].reshape(local_seqs, value_cols, KEY)]
    unnamed x2 -> x0, blocking collectives: 15 us -> none
    psum x2 -> x0, blocking collectives: 11.3 us -> none  [local(): out_squares = lax.psum(jnp.sum(out_rows * out_rows, axis=1), 'dp')]
    all_gather x2 -> x0, blocking collectives: 10.5 us -> none  [local(): lax.all_gather(mixed, 'dp', axis=0, tiled=True)]
  transfers between devices with their start and end apart: 12 -> 0, of which waited for: 11 -> 0; matrix products, arithmetic and copies ran while one was open for 16% -> 0% of each run, Pallas kernels for 0% -> 0%
where the time goes in v1:
time: 60.5 us; the launch traced here: 60.3 us
  Pallas kernels  53.6 us (89%)
  local copies, waits for them, and re-layouts  6.04 us (10%)
  between operations  0.64 us (1%)
    pallas_call x1, Pallas kernels, local(): pl.pallas_call(functools.partial(kernel, dp, tp, qk, vw, tile), out_shape...  53.6 us
    unnamed x2, local copies, waits for them, and re-layouts  6.04 us

profile of v1, /device:TPU:0, one launch (start us, length us, event | category | flops | bytes accessed | tf_op | source)
XLA Modules:
  0.0 60.3 jit_solution(15915403178778819911)
XLA Ops:
  0.6 53.6 %shard_map.131 = (bf16[64,1024]{1,0:T(8,128)(2,1)}, f32[2,16,32768]{2,1,0:T(8,128)}) custom-call(bf16[64,1024]{1,0:T(8,128)(2,1)} %tok.1, f32[2,16,32768]{2,1,0:T(8,128)} %st.1, f32[2,1024]{1,0:T(2,128)} %pre.1, bf16[2,1024,256]{2,1,0:T(8,128)(2,1)} %wq.1, bf16[2,1024,256]{2,1,0:T(8,128)(2,1)} %wk.1, bf16[2,1024,512]{2,1,0:T(8,128)(2,1)} %wv.1, ...), custom_call_target="tpu_custom_call" | custom-call | tf_op jit(solution)/shard_map/pallas_call | solution.py:275
  54.3 1.6 %copy.16 = bf16[64,1024]{1,0:T(8,128)(2,1)} copy(bf16[64,1024]{1,0:T(8,128)(2,1)} %get-tuple-element.4) | data formatting | bytes 262144
  55.8 4.5 %copy.17 = f32[2,16,32768]{2,1,0:T(8,128)} copy(f32[2,16,32768]{2,1,0:T(8,128)} %get-tuple-element.5) | data formatting | bytes 8388608

commit v2 on v1

--- a/solution.py
+++ b/solution.py
@@ -22,11 +22,11 @@
 
 def kernel(
     dp, tp, qk, vw, tile,
-    tok, st, pre, wq, wk, wv, wg, wd, bias, hgain, wo, post,
-    hid, sto,
-    W, WO, S, xf, nrm, part, rbuf, sqa, sqb, psum,
-    qd2, dec2, k2, vv, base, sg, mg, obuf, rb, sqo, sqr, xg,
-    wsem, wosem, ssem, osem, sA, rA, sQ, rQ, sB, rB, sC, rC, sR, rR, sG, rG,
+    st, wq, wk, wv, wg, wd, wo, tok_in, pre_in, bias_in, hgain_in, post_in,
+    hid, S,
+    tok, pre, bias, hgain, post, W, WO, xf, nrm, part, rbuf, sqa, sqb, psum,
+    qd2, dec2, k2, vv, base, sg, mg, obuf, rb, sqr, xg,
+    small, wsem, wosem, ssem, sA, rA, sQ, rQ, sB, rB, sC, rC, sR, rR, sG, rG,
 ):
     me_dp = lax.axis_index("dp")
     me_tp = lax.axis_index("tp")
@@ -47,10 +47,30 @@
     def tp_peer(k):
         return lax.rem(me_tp + k, tp)
 
-    for k in range(1, dp):
-        pl.semaphore_signal(pltpu.get_barrier_semaphore(), inc=1, device_id={"dp": dp_peer(k)}, device_id_type=MESH)
-    for k in range(1, tp):
-        pl.semaphore_signal(pltpu.get_barrier_semaphore(), inc=1, device_id={"tp": tp_peer(k)}, device_id_type=MESH)
+    every = dp * tp
+    me = me_tp * dp + me_dp
+
+    small_copies = [
+        pltpu.make_async_copy(src, dst, small.at[n])
+        for n, (src, dst) in enumerate(
+            ((tok_in, tok), (pre_in, pre), (bias_in, bias), (hgain_in, hgain), (post_in, post))
+        )
+    ]
+    dp_peers = [me_dp] + [dp_peer(k) for k in range(1, dp)]
+
+    def visit(act):
+        def step(kt, c):
+            target = tp_peer(kt)
+            for kd in range(dp):
+                act(kt, kd, {"tp": target, "dp": dp_peers[kd]})
+            return c
+
+        for kd in range(1, dp):
+            act(0, kd, {"dp": dp_peers[kd]})
+        lax.fori_loop(1, tp, step, 0)
+
+    def greet(kt, kd, target):
+        pl.semaphore_signal(pltpu.get_barrier_semaphore(), inc=1, device_id=target, device_id_type=MESH)
 
     def weight_copy(b, n):
         ref, at, width = sections[n]
@@ -59,19 +79,14 @@
     def state_in(b):
         return pltpu.make_async_copy(st.at[b], S.at[b], ssem.at[b])
 
-    def state_out(b):
-        return pltpu.make_async_copy(S.at[b], sto.at[b], osem.at[b])
-
     def wo_copy(b):
         return pltpu.make_async_copy(wo.at[b], WO.at[b], wosem.at[b])
 
-    for b in range(2):
-        for n in range(5):
-            weight_copy(b, n).start()
-        state_in(b).start()
-        wo_copy(b).start()
-
-    xf[...] = tok[...].astype(F32)
+    for copy in small_copies:
+        copy.start()
+    for n in range(5):
+        weight_copy(0, n).start()
+    visit(greet)
     lane = lax.broadcasted_iota(jnp.int32, (LANES, LANES), 1)
     depth = lax.broadcasted_iota(jnp.int32, (LANES, LANES), 0)
     reducer = (depth // KEY == lane % 2).astype(F32).astype(BF16)
@@ -79,8 +94,7 @@
     pair_of = lane_row // 2
     low_half = lane_row < KEY
     pairs = VAL // 2
-
-    pl.semaphore_wait(pltpu.get_barrier_semaphore(), dp - 1 + tp - 1)
+    diagonal = lax.broadcasted_iota(jnp.int32, (orows, LANES), 0) == lax.broadcasted_iota(jnp.int32, (orows, LANES), 1)
 
     def remote(src, dst, send, recv, axis, peer):
         return pltpu.make_async_remote_copy(
@@ -94,18 +108,26 @@
     def copy_Q(b, k):
         return remote(sqa.at[b, dp_peer(k)], sqb.at[b, k], sQ.at[b, k], rQ.at[b, k], "dp", dp_peer(k))
 
-    def copy_B(b, k):
-        return remote(mg.at[b, me_dp], mg.at[b, me_dp], sB.at[b, k], rB.at[b, k], "dp", dp_peer(k))
-
-    def wait_B(b, k):
-        src = lax.rem(me_dp + dp - k, dp)
-        remote(mg.at[b, src], mg.at[b, src], sB.at[b, k], rB.at[b, k], "dp", dp_peer(k)).wait_recv()
+    def copy_B(b, h, k):
+        own = mg.at[b, me_dp, h]
+        return remote(own, own, sB.at[b, h, k], rB.at[b, h, k], "dp", dp_peer(k))
+
+    def wait_B(b, h, k):
+        src = mg.at[b, lax.rem(me_dp + dp - k, dp), h]
+        remote(src, src, sB.at[b, h, k], rB.at[b, h, k], "dp", dp_peer(k)).wait_recv()
 
     def copy_C(b, k):
         return remote(obuf.at[b, tp_peer(k)], rb.at[b, k], sC.at[b, k], rC.at[b, k], "tp", tp_peer(k))
 
-    def copy_R(b, k):
-        return remote(sqo.at[b], sqr.at[b, k], sR.at[b, k], rR.at[b, k], "dp", dp_peer(k))
+    def send_R(b, kt, kd, target):
+        pltpu.make_async_remote_copy(
+            src_ref=sqr.at[b, 0], dst_ref=sqr.at[b, kt * dp + kd], send_sem=sR.at[b], recv_sem=rR.at[b],
+            device_id=target, device_id_type=MESH,
+        ).start()
+
+    def all_R(b):
+        others = sqr.at[b, pl.ds(1, every - 1)]
+        return remote(others, others, sR.at[b], rR.at[b], "dp", dp_peer(1))
 
     def copy_G(b, k):
         return remote(xg.at[b, me_tp], xg.at[b, me_tp], sG.at[b, k], rG.at[b, k], "tp", tp_peer(k))
@@ -114,26 +136,45 @@
         src = lax.rem(me_tp + tp - k, tp)
         remote(xg.at[b, src], xg.at[b, src], sG.at[b, k], rG.at[b, k], "tp", tp_peer(k)).wait_recv()
 
-    def block(b, carry):
+    first_tile = [at // tile for _, at, _ in sections]
+
+    def send_tile(b, t):
+        for k in range(1, dp):
+            copy_A(b, t, k).start()
+
+    def project(b, send):
         x = xf[...]
         squares = jnp.sum(x * x, axis=1, keepdims=True)
         sqa[b] = jnp.broadcast_to(squares, (seqs, LANES)).reshape(dp, rows, LANES)
         nrm[...] = (x * pre[pl.ds(b, 1), :]).astype(BF16)
-        for k in range(1, dp):
-            copy_Q(b, k).start()
-        for n in range(5):
-            weight_copy(b, n).wait()
-
-        def project(t, c):
-            cols = pl.ds(pl.multiple_of(t * tile, tile), tile)
-            y = jnp.dot(nrm[...], W[b, :, cols], preferred_element_type=F32)
+        if send:
+            for k in range(1, dp):
+                copy_Q(b, k).start()
+        for t in range(tiles):
+            if t in first_tile:
+                weight_copy(b, first_tile.index(t)).wait()
+            y = jnp.dot(nrm[...], W[b, :, t * tile : (t + 1) * tile], preferred_element_type=F32)
             part[b, t] = y.reshape(dp, rows, tile).astype(BF16)
-            for k in range(1, dp):
-                copy_A(b, t, k).start()
-            return c
-
-        lax.fori_loop(0, tiles, project, 0)
-
+            if send:
+                send_tile(b, t)
+
+    for copy in small_copies:
+        copy.wait()
+    xf[...] = tok[...].astype(F32)
+    project(0, False)
+    state_in(0).start()
+    wo_copy(0).start()
+    for n in range(5):
+        weight_copy(1, n).start()
+    state_in(1).start()
+    wo_copy(1).start()
+    pl.semaphore_wait(pltpu.get_barrier_semaphore(), every - 1)
+    for k in range(1, dp):
+        copy_Q(0, k).start()
+    for t in range(tiles):
+        send_tile(0, t)
+
+    def block(b, carry):
         total_sq = sqa[b, me_dp]
         for k in range(1, dp):
             copy_Q(b, k).wait_recv()
@@ -185,16 +226,18 @@
             read = acc * KEY ** (-0.5)
             mean = jnp.mean(read * read, axis=1, keepdims=True)
             mixed = read * lax.rsqrt(mean + epsilon) * hgain[pl.ds(b, 1), :] * sg[h]
-            mg[b, me_dp, :, pl.ds(pl.multiple_of(h * VAL, VAL), VAL)] = mixed.astype(BF16)
+            mg[b, me_dp, h] = mixed.astype(BF16)
+            for k in range(1, dp):
+                copy_B(b, h, k).start()
             return c
 
         lax.fori_loop(0, heads, readout, 0)
-        for k in range(1, dp):
-            copy_B(b, k).start()
         wo_copy(b).wait()
-        for k in range(1, dp):
-            wait_B(b, k)
-        out = jnp.dot(mg[b].reshape(seqs, vw), WO[b], preferred_element_type=F32)
+        for h in range(heads):
+            for k in range(1, dp):
+                wait_B(b, h, k)
+        mixed_all = jnp.concatenate([mg[b, :, h].reshape(seqs, VAL) for h in range(heads)], axis=1)
+        out = jnp.dot(mixed_all, WO[b], preferred_element_type=F32)
         obuf[b] = out.reshape(tp, orows, out.shape[1]).astype(BF16)
         for k in range(1, tp):
             copy_C(b, k).start()
@@ -209,33 +252,42 @@
             return c
 
         lax.fori_loop(0, heads, update, 0)
-        state_out(b).start()
 
         total = obuf[b, me_tp].astype(F32)
         for k in range(1, tp):
             copy_C(b, k).wait_recv()
             total = total + rb[b, k].astype(F32)
         own_sq = jnp.broadcast_to(jnp.sum(total * total, axis=1, keepdims=True), (orows, LANES))
-        sqo[b] = own_sq
-        for k in range(1, dp):
-            copy_R(b, k).start()
-        mine = xf[pl.ds(pl.multiple_of(me_tp * orows, orows), orows), :]
-        gained = total * post[pl.ds(b, 1), :]
-        for k in range(1, dp):
-            copy_R(b, k).wait_recv()
-            own_sq = own_sq + sqr[b, k]
-        out_scale = lax.rsqrt(own_sq[:, :1] / feats + epsilon)
-        xg[b, me_tp] = (mine + gained * out_scale).astype(BF16)
-        for k in range(1, tp):
+        sqr[b, 0] = jnp.sum(jnp.where(diagonal, own_sq, 0.0), axis=0, keepdims=True)
+        xg[b, me_tp] = total.astype(BF16)
+
+        for k in range(tp - 1, 0, -1):
             copy_G(b, k).start()
+        visit(functools.partial(send_R, b))
+        all_R(b).wait_recv()
         for k in range(1, tp):
             wait_G(b, k)
-        xf[...] = xg[b].astype(F32).reshape(seqs, xf.shape[1])
+
+        for t in range(tp):
+            from_tp = lax.rem(me_tp + tp - t, tp) * dp
+            out_sq = jnp.zeros((1, LANES), F32)
+            for d in range(dp):
+                out_sq = out_sq + sqr[b, from_tp + lax.rem(me_dp + dp - d, dp)]
+            spread = jnp.where(diagonal, jnp.broadcast_to(out_sq, (orows, LANES)), 0.0)
+            out_scale = lax.rsqrt(jnp.sum(spread, axis=1, keepdims=True) / feats + epsilon)
+            here = pl.ds(t * orows, orows)
+            fresh = xf[here, :] + xg[b, t].astype(F32) * out_scale * post[pl.ds(b, 1), :]
+            xf[here, :] = fresh.astype(BF16).astype(F32)
+
+        @pl.when(b == 0)
+        def _():
+            project(1, True)
 
         for k in range(1, dp):
             copy_Q(b, k).wait_send()
-            copy_B(b, k).wait_send()
-            copy_R(b, k).wait_send()
+            for h in range(heads):
+                copy_B(b, h, k).wait_send()
+        all_R(b).wait_send()
 
         def drain(t, c):
             for k in range(1, dp):
@@ -250,8 +302,16 @@
 
     lax.fori_loop(0, 2, block, 0)
     hid[...] = xf[...].astype(BF16)
+
+
+def store_kernel(hid, st, hid_out, st_out, sems):
+    copies = [pltpu.make_async_copy(hid, hid_out, sems.at[0])]
     for b in range(2):
-        state_out(b).wait()
+        copies.append(pltpu.make_async_copy(st.at[b], st_out.at[b], sems.at[1 + b]))
+    for copy in copies:
+        copy.start()
+    for copy in copies:
+        copy.wait()
 
 
 def solution(mesh):
@@ -268,22 +328,23 @@
         total = 3 * pad(qk) + 2 * vw
         tile = 2 * LANES if total % (2 * LANES) == 0 and pad(qk) % (2 * LANES) == 0 else LANES
         tiles = total // tile
+        arrays = tuple(
+            pltpu.with_memory_space_constraint(array, pltpu.HBM)
+            for array in (st, wq, wk, wv, wg, wd, wo, tok, pre, bias, hgain, post)
+        )
         vmem = pl.BlockSpec(memory_space=pltpu.VMEM)
         hbm = pl.BlockSpec(memory_space=pl.ANY)
         dma = pltpu.SemaphoreType.DMA
         per_head = pltpu.VMEM((heads, rows, LANES), F32)
-        return pl.pallas_call(
+        hid, new_state = pl.pallas_call(
             functools.partial(kernel, dp, tp, qk, vw, tile),
-            out_shape=(
-                jax.ShapeDtypeStruct(tok.shape, BF16),
-                jax.ShapeDtypeStruct(st.shape, F32),
-            ),
-            in_specs=[vmem, hbm, vmem, hbm, hbm, hbm, hbm, hbm, vmem, vmem, hbm, vmem],
-            out_specs=(vmem, hbm),
+            out_shape=(pltpu.VMEM(tok.shape, BF16), pltpu.VMEM(st.shape, F32)),
+            in_specs=[hbm] * 12,
+            out_specs=(vmem, vmem),
             scratch_shapes=[
+                *(pltpu.VMEM(a.shape, a.dtype) for a in (tok, pre, bias, hgain, post)),
                 pltpu.VMEM((2, width, total), BF16),
                 pltpu.VMEM((2,) + wo.shape[1:], BF16),
-                pltpu.VMEM(st.shape, F32),
                 pltpu.VMEM((seqs, width), F32),
                 pltpu.VMEM((seqs, width), BF16),
                 pltpu.VMEM((2, tiles, dp, rows, tile), BF16),
@@ -292,24 +353,33 @@
                 pltpu.VMEM((2, dp, rows, LANES), F32),
                 pltpu.VMEM((tiles, rows, tile), F32),
                 per_head, per_head, per_head, per_head, per_head, per_head,
-                pltpu.VMEM((2, dp, rows, vw), BF16),
+                pltpu.VMEM((2, dp, heads, rows, VAL), BF16),
                 pltpu.VMEM((2, tp, orows, width), BF16),
                 pltpu.VMEM((2, tp, orows, width), BF16),
-                pltpu.VMEM((2, orows, LANES), F32),
-                pltpu.VMEM((2, dp, orows, LANES), F32),
+                pltpu.VMEM((2, dp * tp, 1, LANES), F32),
                 pltpu.VMEM((2, tp, orows, width), BF16),
-                dma((2, 5)), dma((2,)), dma((2,)), dma((2,)),
+                dma((5,)), dma((2, 5)), dma((2,)), dma((2,)),
                 dma((2, tiles, dp)), dma((2, tiles, dp)),
                 dma((2, dp)), dma((2, dp)),
-                dma((2, dp)), dma((2, dp)),
+                dma((2, heads, dp)), dma((2, heads, dp)),
                 dma((2, tp)), dma((2, tp)),
-                dma((2, dp)), dma((2, dp)),
+                dma((2,)), dma((2,)),
                 dma((2, tp)), dma((2, tp)),
             ],
             compiler_params=pltpu.CompilerParams(
-                collective_id=0, has_side_effects=True, vmem_limit_bytes=60 * 2**20
+                collective_id=0, has_side_effects=True, vmem_limit_bytes=24 * 2**20
             ),
-        )(tok, st, pre, wq, wk, wv, wg, wd, bias, hgain, wo, post)
+        )(*arrays)
+        return pl.pallas_call(
+            store_kernel,
+            out_shape=(
+                jax.ShapeDtypeStruct(tok.shape, BF16),
+                jax.ShapeDtypeStruct(st.shape, F32),
+            ),
+            in_specs=[hbm, hbm],
+            out_specs=(hbm, hbm),
+            scratch_shapes=[dma((3,))], compiler_params=pltpu.CompilerParams(vmem_limit_bytes=2**20),
+        )(pltpu.with_memory_space_constraint(hid, pltpu.VMEM), pltpu.with_memory_space_constraint(new_state, pltpu.VMEM))
 
     in_specs = (
         P(None, "dp"),

time: 60.5 us -> 53.2 us (0.88)
  local copies, waits for them, and re-layouts: 6.04 us -> 0 us
  Pallas kernels: 53.6 us -> 52.5 us
    unnamed x2 -> x0, local copies, waits for them, and re-layouts: 6.04 us -> none
    pallas_call x1, Pallas kernels: 53.6 us -> 50.4 us  [local(): pl.pallas_call(functools.partial(kernel, dp, tp, qk, vw, tile), out_shape...]
    pallas_call x0 -> x1, Pallas kernels: none -> 2.08 us  [local(): pl.pallas_call(store_kernel, out_shape=(jax.ShapeDtypeStruct(tok.shape, B...]
where the time goes in v2:
time: 53.2 us; the launch traced here: 53.1 us
  Pallas kernels  52.5 us (99%)
  between operations  0.64 us (1%)
    pallas_call x1, Pallas kernels, local(): pl.pallas_call(functools.partial(kernel, dp, tp, qk, vw, tile), out_shape...  50.4 us
    pallas_call x1, Pallas kernels, local(): pl.pallas_call(store_kernel, out_shape=(jax.ShapeDtypeStruct(tok.shape, B...  2.08 us

profile of v2, /device:TPU:0, one launch (start us, length us, event | category | flops | bytes accessed | tf_op | source)
XLA Modules:
  0.0 53.1 jit_solution(12012520350451954195)
XLA Ops:
  0.6 50.4 %shard_map.131 = (bf16[64,1024]{1,0:T(8,128)(2,1)S(1)}, f32[2,16,32768]{2,1,0:T(8,128)S(1)}) custom-call(f32[2,16,32768]{2,1,0:T(8,128)} %st.1, bf16[2,1024,256]{2,1,0:T(8,128)(2,1)} %wq.1, bf16[2,1024,256]{2,1,0:T(8,128)(2,1)} %wk.1, bf16[2,1024,512]{2,1,0:T(8,128)(2,1)} %wv.1, bf16[2,1024,512]{2,1,0:T(8,128)(2,1)} %wg.1, bf16[2,1024,256]{2,1,0:T(8,128)(2,1)} %wd.1, ...), custom_call_target="tpu_custom_call" | custom-call | tf_op jit(solution)/shard_map/pallas_call | solution.py:339
  51.0 2.1 %shard_map.132 = (bf16[64,1024]{1,0:T(8,128)(2,1)}, f32[2,16,32768]{2,1,0:T(8,128)}) custom-call(bf16[64,1024]{1,0:T(8,128)(2,1)S(1)} %get-tuple-element.4.hid, f32[2,16,32768]{2,1,0:T(8,128)S(1)} %get-tuple-element.5.st), custom_call_target="tpu_custom_call" | custom-call | tf_op jit(solution)/shard_map/pallas_call | solution.py:373
